TPU v7x, 256 devices: a 2x2x32 block of a 4x16x32 slice. The times are simulated.
256 devices in a mesh: grp: 4 (over y, x), ep: 32 (over z), tp: 2 (over core).
Axes of the slice: x: 2, y: 2, z: 32, core: 2. Of those that a mesh axis runs over, the one named last changes fastest.
The devices are a block of a 4x16x32 slice.
Arguments:
- tokens: bfloat16 [65536, 2048], P(('grp', 'ep', 'tp')), parts along dimension 0, may hold values from -6 to 6
- norm_gain: float32 [2048], replicated, may hold values from 0.1 to 1.9
- route_ids: int32 [65536, 2], P(('grp', 'ep', 'tp')), parts along dimension 0, may hold values from 0 to 31, as said below
- route_weights: float32 [65536, 2], P(('grp', 'ep', 'tp')), parts along dimension 0, may hold values from 0.1 to 1
- w_gate: bfloat16 [32, 2048, 512], P('ep', None, 'tp'), may hold values from -0.125 to 0.125
- w_up: bfloat16 [32, 2048, 512], P('ep', None, 'tp'), may hold values from -0.125 to 0.125
- w_down: bfloat16 [32, 512, 2048], P('ep', 'tp'), may hold values from -0.25 to 0.25
Outputs:
- mixed: bfloat16 [65536, 2048], P(('grp', 'ep', 'tp')), parts along dimension 0
There are 4 independent parts, one for each index of `grp`. A program takes and returns all parts, laid end to end along the dimension named above; an argument that names none is the same for every part. Nothing has to cross between parts.
Inputs may be any that keep to these rules, and one draw needn't show every extreme that they name: `route_ids`: the 2 experts of a token are different and lie in one group of 8 consecutive experts. Among the tokens of one device (aligned blocks of 256 tokens) no expert is named more than 32 times, and in every such block some expert is named exactly 32 times.
All inputs are finite; a program needn't handle non-finite values.
Results may differ from a plain program's by a relative error of at most 0.007.
Values may be sent and summed in bfloat16 or wider, within the bound.
A program may use at most 128 MiB of HBM per device.

v0:
```python
import functools

import jax
import jax.numpy as jnp
from jax import lax
from jax.experimental import pallas as pl
from jax.experimental.pallas import tpu as pltpu
from jax.sharding import PartitionSpec as P

GROUPS = 4

epsilon = 1e-06

CHUNK = 8
LAG = 5
CHUNKS = 232
BIAS = 6
SLOTS = 8
LANES = 128


def send_back(result):
    return lax.all_to_all(result, "ep", split_axis=0, concat_axis=0, tiled=True)


def ring_setup(others=()):
    ep = lax.axis_size("ep")
    me = lax.axis_index("ep")
    up, down = lax.rem(me + 1, ep), lax.rem(me + ep - 1, ep)
    peers = [{"ep": up}, {"ep": down}] + list(others)
    barrier = pltpu.get_barrier_semaphore()
    for peer in peers:
        pl.semaphore_signal(
            barrier, inc=1, device_id=peer, device_id_type=pl.DeviceIdType.MESH
        )
    pl.semaphore_wait(barrier, len(peers))
    return up, down


def chunk_copy(send, land, send_sem, recv_sem, peer, way, slot, chunk):
    return pltpu.make_async_remote_copy(
        src_ref=send.at[way, slot],
        dst_ref=land.at[way, chunk],
        send_sem=send_sem.at[way, slot],
        recv_sem=recv_sem.at[way, chunk],
        device_id={"ep": peer},
        device_id_type=pl.DeviceIdType.MESH,
    )


def ring_stream(peers, order, build, keep, send, land, send_sem, recv_sem):
    def receive(step):
        for way in (0, 1):
            chunk = order(step)
            chunk_copy(send, land, send_sem, recv_sem, peers[way], way, 0, chunk).wait_recv()
            keep(way, chunk)

    def drain(step):
        slot = lax.rem(step, SLOTS)
        for way in (0, 1):
            chunk_copy(
                send, land, send_sem, recv_sem, peers[way], way, slot, order(step)
            ).wait_send()

    def body(step, carry):
        slot = lax.rem(step, SLOTS)

        @pl.when(step >= LAG)
        def _():
            receive(step - LAG)

        @pl.when(step >= SLOTS)
        def _():
            drain(step - SLOTS)

        for way in (0, 1):
            build(way, slot, order(step))
        for way in (0, 1):
            chunk_copy(
                send, land, send_sem, recv_sem, peers[way], way, slot, order(step)
            ).start()
        return carry

    lax.fori_loop(0, CHUNKS, body, 0)
    for step in range(CHUNKS - LAG, CHUNKS):
        receive(step)
    for step in range(CHUNKS - SLOTS, CHUNKS):
        drain(step)


def half_copies(halves, wholes, half_sem, own_sem, half, other):
    remote, local = [], []
    for index, (part, whole) in enumerate(zip(halves, wholes)):
        if part.shape[0] == whole.shape[0]:
            width = part.shape[1]
            place = whole.at[:, pl.ds(pl.multiple_of(half * width, width), width)]
        else:
            depth = part.shape[0]
            place = whole.at[pl.ds(pl.multiple_of(half * depth, depth), depth)]
        remote.append(
            pltpu.make_async_remote_copy(
                src_ref=part,
                dst_ref=place,
                send_sem=half_sem.at[0, index],
                recv_sem=half_sem.at[1, index],
                device_id=other,
                device_id_type=pl.DeviceIdType.MESH,
            )
        )
        local.append(pltpu.make_async_copy(part, place, own_sem.at[index]))
    return remote, local


def dispatch_kernel(
    pick_ref,
    expert_ref,
    own_ref,
    gate_half,
    up_half,
    down_half,
    out_ref,
    gate_whole,
    up_whole,
    down_whole,
    store,
    send,
    land,
    send_sem,
    recv_sem,
    half_sem,
    own_sem,
):
    rows = CHUNKS * CHUNK
    half = lax.axis_index("tp")
    other = {"tp": 1 - half}
    peers = ring_setup([other])
    halves = (gate_half, up_half, down_half)
    wholes = (gate_whole, up_whole, down_whole)
    remote, local = half_copies(halves, wholes, half_sem, own_sem, half, other)
    for copy in remote + local:
        copy.start()
    own_rows = own_ref.shape[0]

    def take(block, carry):
        at = pl.multiple_of(block * CHUNK, CHUNK)
        store[pl.ds(2 * rows + at, CHUNK)] = own_ref[pl.ds(at, CHUNK)]
        return carry

    lax.fori_loop(0, own_rows // CHUNK, take, 0)
    store[pl.ds(2 * rows + own_rows, 1)] = jnp.zeros((1,) + own_ref.shape[1:], own_ref.dtype)

    def keep(way, chunk):
        store[pl.ds(way * rows + chunk * CHUNK, CHUNK)] = land[way, chunk]

    def build(way, slot, chunk):
        for row in range(CHUNK):
            send[way, slot, row] = store[pick_ref[way, chunk * CHUNK + row]]

    ring_stream(peers, lambda step: step, build, keep, send, land, send_sem, recv_sem)

    def gather(block, carry):
        for row in range(CHUNK):
            at = block * CHUNK + row
            out_ref[at] = store[expert_ref[at]]
        return carry

    lax.fori_loop(0, out_ref.shape[0] // CHUNK, gather, 0)
    for copy in remote + local:
        copy.wait()


def collect_kernel(
    result_ref,
    onward_ref,
    final_ref,
    result,
    out_ref,
    store,
    send,
    land,
    send_sem,
    recv_sem,
    load_sem,
):
    rows = CHUNKS * CHUNK
    load = pltpu.make_async_copy(
        result, store.at[pl.ds(2 * rows + CHUNK, result.shape[0])], load_sem
    )
    load.start()
    up, down = ring_setup()
    store[pl.ds(2 * rows, 1)] = jnp.zeros((1,) + store.shape[1:], store.dtype)
    load.wait()

    def keep(way, chunk):
        store[pl.ds(way * rows + chunk * CHUNK, CHUNK)] = land[way, chunk]

    def build(way, slot, chunk):
        for row in range(CHUNK):
            at = chunk * CHUNK + row
            here = store[result_ref[way, at]].astype(jnp.float32)
            beyond = store[onward_ref[way, at]].astype(jnp.float32)
            send[way, slot, row] = (here + beyond).astype(send.dtype)

    ring_stream(
        (down, up),
        lambda step: CHUNKS - 1 - step,
        build,
        keep,
        send,
        land,
        send_sem,
        recv_sem,
    )

    def finish(block, carry):
        for row in range(CHUNK):
            at = block * CHUNK + row
            total = store[final_ref[2, at]].astype(jnp.float32)
            for way in (0, 1):
                total = total + store[final_ref[way, at]].astype(jnp.float32)
            out_ref[at] = total.astype(out_ref.dtype)
        return carry

    lax.fori_loop(0, out_ref.shape[0] // CHUNK, finish, 0)


def ring_scratch(store_rows, row_shape):
    return [
        pltpu.VMEM((store_rows,) + row_shape, jnp.bfloat16),
        pltpu.VMEM((2, SLOTS, CHUNK) + row_shape, jnp.bfloat16),
        pltpu.VMEM((2, CHUNKS, CHUNK) + row_shape, jnp.bfloat16),
        pltpu.SemaphoreType.DMA((2, SLOTS)),
        pltpu.SemaphoreType.DMA((2, CHUNKS)),
    ]


def ring_params(collective_id):
    return pltpu.CompilerParams(
        collective_id=collective_id, has_side_effects=True, vmem_limit_bytes=60 * 1024 * 1024
    )


SMEM = pl.BlockSpec(memory_space=pltpu.SMEM)
VMEM = pl.BlockSpec(memory_space=pltpu.VMEM)
ANY = pl.BlockSpec(memory_space=pl.ANY)


def dispatch(pick, expert, own, halves):
    row_shape = own.shape[1:]
    gate_half, up_half, down_half = halves
    wholes = [
        jax.ShapeDtypeStruct((part.shape[0], part.shape[1] * 2), part.dtype)
        for part in (gate_half, up_half)
    ] + [jax.ShapeDtypeStruct((down_half.shape[0] * 2, down_half.shape[1]), down_half.dtype)]
    return pl.pallas_call(
        dispatch_kernel,
        out_shape=[jax.ShapeDtypeStruct((expert.shape[0],) + row_shape, jnp.bfloat16)] + wholes,
        in_specs=[SMEM, SMEM, VMEM, ANY, ANY, ANY],
        out_specs=[VMEM, ANY, ANY, ANY],
        scratch_shapes=ring_scratch(2 * CHUNKS * CHUNK + own.shape[0] + 1, row_shape)
        + [pltpu.SemaphoreType.DMA((2, 3)), pltpu.SemaphoreType.DMA((3,))],
        compiler_params=ring_params(0),
        name="dispatch",
    )(pick, expert, own, *halves)


def collect(result_pick, onward, final, result):
    row_shape = result.shape[1:]
    return pl.pallas_call(
        collect_kernel,
        out_shape=jax.ShapeDtypeStruct((final.shape[1],) + row_shape, jnp.bfloat16),
        in_specs=[SMEM, SMEM, SMEM, ANY],
        out_specs=VMEM,
        scratch_shapes=ring_scratch(2 * CHUNKS * CHUNK + CHUNK + result.shape[0], row_shape)
        + [pltpu.SemaphoreType.DMA],
        compiler_params=ring_params(1),
        name="collect",
    )(result_pick, onward, final, result)


def starts_kernel(steps, counts_ref, starts_ref, lives_ref):
    for way, shift in ((0, 1), (1, LANES - 1)):
        start = jnp.zeros((1, LANES), jnp.int32)
        live = counts_ref[way * steps : way * steps + 1]
        for distance in range(steps):
            if distance:
                start = jnp.maximum(
                    start + live, pltpu.roll(start, shift, axis=1) + LAG * CHUNK
                )
                at = way * steps + distance
                live = pltpu.roll(counts_ref[at : at + 1], shift * distance % LANES, axis=1)
            starts_ref[way * steps + distance : way * steps + distance + 1] = start
            lives_ref[way * steps + distance : way * steps + distance + 1] = live


def stream_starts(counts, steps):
    shape = jax.ShapeDtypeStruct(counts.shape, jnp.int32)
    return pl.pallas_call(
        functools.partial(starts_kernel, steps),
        out_shape=[shape, shape],
        in_specs=[VMEM],
        out_specs=[VMEM, VMEM],
        name="starts",
    )(counts)


def plan_routes(route_ids, route_weights, capacity):
    ep = lax.axis_size("ep")
    me = lax.axis_index("ep")
    tokens = route_ids.shape[0]
    steps = ep // 2 + ep // GROUPS
    low = jnp.min(route_ids, axis=1)
    high = jnp.max(route_ids, axis=1)
    ahead = jnp.maximum((low - me) % ep, (high - me) % ep)
    behind = jnp.maximum((me - low) % ep, (me - high) % ep)
    inside = (low <= me) & (me <= high)
    upward = ahead <= behind
    bias = jnp.arange(-BIAS, BIAS + 1, dtype=jnp.int32)[:, None]
    try_up = (ahead - behind)[None, :] <= bias
    ways = [
        jnp.where(inside, high - me, jnp.where(try_up, ahead, 0)),
        jnp.where(inside, me - low, jnp.where(try_up, 0, behind)),
    ]
    cost = jnp.maximum(jnp.sum(ways[0], axis=1), jnp.sum(ways[1], axis=1))[:, None]
    cost = (cost * 16 + jnp.abs(bias)) * 2 + (bias > 0).astype(jnp.int32)
    best = jnp.sum(jnp.where(cost == jnp.min(cost), bias, 0))
    upward = (ahead - behind) <= best
    reach = jnp.stack(
        [
            jnp.where(inside, high - me, jnp.where(upward, ahead, 0)),
            jnp.where(inside, me - low, jnp.where(upward, 0, behind)),
        ]
    )
    position = jnp.arange(tokens, dtype=jnp.int32)
    before = position[None, :] < position[:, None]
    further = (reach[:, None, :] > reach[:, :, None]) | (
        (reach[:, None, :] == reach[:, :, None]) & before[None]
    )
    rank = jnp.sum(further.astype(jnp.int32), axis=2)
    alive = jnp.sum(
        (reach[:, :, None] > jnp.arange(steps, dtype=jnp.int32)[None, None, :]).astype(jnp.int32),
        axis=1,
    )
    same = jnp.zeros((tokens, route_ids.shape[1]), jnp.int32)
    for column in range(route_ids.shape[1]):
        match = route_ids[:, :, None] == route_ids[None, None, :, column].reshape(1, 1, tokens)
        same = same + jnp.sum((match & before[:, None, :]).astype(jnp.int32), axis=2)
    target = route_ids * capacity + same
    goes_up = jnp.where(inside[:, None], route_ids > me, upward[:, None])
    code = jnp.where(goes_up, rank[0][:, None], tokens + rank[1][:, None])
    code = jnp.where(route_ids == me, 2 * tokens + position[:, None], code)
    slots = jnp.arange(ep * capacity, dtype=jnp.int32)
    sent_code = jnp.zeros((ep * capacity,), jnp.float32)
    sent_weight = jnp.zeros((ep * capacity,), jnp.float32)
    for column in range(route_ids.shape[1]):
        hit = slots[:, None] == target[None, :, column]
        sent_code = sent_code + jnp.sum(
            jnp.where(hit, (code[:, column] + 1).astype(jnp.float32)[None, :], 0.0), axis=1
        )
        sent_weight = sent_weight + jnp.sum(
            jnp.where(hit, route_weights[:, column][None, :], 0.0), axis=1
        )
    counts = alive.astype(jnp.float32).reshape(1, 2 * steps)
    message = jnp.concatenate(
        [
            sent_code.reshape(ep, capacity),
            sent_weight.reshape(ep, capacity),
            jnp.broadcast_to(counts, (ep, 2 * steps)),
        ],
        axis=1,
    )
    message = jnp.pad(message, ((0, 0), (0, LANES - message.shape[1])))
    return message, reach, rank, target, steps


def lookup(table, index, size):
    choice = index[..., None] == jnp.arange(size, dtype=jnp.int32)
    return jnp.sum(jnp.where(choice, table, 0), axis=-1)


def plan_streams(arrived, reach, rank, target, route_ids, steps, capacity, starts_of):
    ep = lax.axis_size("ep")
    me = lax.axis_index("ep")
    rows = CHUNKS * CHUNK
    tokens = rank.shape[1]
    codes = arrived[:, :capacity].astype(jnp.int32) - 1
    counts = arrived[:, 2 * capacity : 2 * capacity + 2 * steps].astype(jnp.int32)
    counts = jnp.tile(counts.T, (1, LANES // ep))
    starts, lives = starts_of(counts, steps)
    starts = starts.reshape(2, steps, LANES)
    lives = lives.reshape(2, steps, LANES)
    fits = jnp.max(jnp.where(lives > 0, starts + lives, 0)) <= rows

    column = jnp.arange(LANES, dtype=jnp.int32)

    def at_device(table, device):
        return jnp.sum(jnp.where(column[None, None, :] == device[:, None, None], table, 0), axis=2)

    spot = jnp.stack([me, me])
    previous = jnp.stack([(me + ep - 1) % ep, (me + 1) % ep])
    out_start, out_live = at_device(starts, spot), at_device(lives, spot)
    in_start, in_live = at_device(starts, previous), at_device(lives, previous)
    way_base = (jnp.arange(2, dtype=jnp.int32) * rows)[:, None]
    place = jnp.arange(rows, dtype=jnp.int32)

    def locate(start, live):
        distance = (
            jnp.sum((place[None, :, None] >= start[:, None, :]).astype(jnp.int32), axis=2) - 1
        )
        choice = distance[:, :, None] == jnp.arange(steps, dtype=jnp.int32)
        within = place[None] - jnp.sum(jnp.where(choice, start[:, None, :], 0), axis=2)
        valid = within < jnp.sum(jnp.where(choice, live[:, None, :], 0), axis=2)
        return choice, within, valid

    own_list = jnp.sum(
        jnp.where(
            rank[:, None, :] == jnp.arange(tokens, dtype=jnp.int32)[None, :, None],
            jnp.arange(tokens, dtype=jnp.int32)[None, None, :],
            0,
        ),
        axis=2,
    )
    own_list = jnp.pad(own_list, ((0, 0), (0, rows - tokens)))
    zero_row = 2 * rows + tokens
    choice, within, valid = locate(out_start, out_live)
    shifted = jnp.concatenate([jnp.zeros((2, 1), jnp.int32), in_start[:, :-1]], axis=1)
    source = way_base + within + jnp.sum(jnp.where(choice, shifted[:, None, :], 0), axis=2)
    source = jnp.where(choice[:, :, 0], 2 * rows + own_list, source)
    pick = jnp.clip(jnp.where(valid, source, zero_row), 0, zero_row)

    none_row = 2 * rows
    choice, within, valid = locate(in_start, in_live)
    next_start = jnp.concatenate([out_start[:, 1:], jnp.zeros((2, 1), jnp.int32)], axis=1)
    next_live = jnp.concatenate([out_live[:, 1:], jnp.zeros((2, 1), jnp.int32)], axis=1)
    goes_on = valid & (within < jnp.sum(jnp.where(choice, next_live[:, None, :], 0), axis=2))
    onward = way_base + within + jnp.sum(jnp.where(choice, next_start[:, None, :], 0), axis=2)
    onward = jnp.clip(jnp.where(goes_on, onward, none_row), 0, none_row)

    source_of = jnp.arange(ep, dtype=jnp.int32)
    far = jnp.stack([(me - 1 - source_of) % ep, (source_of - me - 1) % ep])
    base = jnp.stack([lookup(in_start[way], far[way], steps) for way in (0, 1)])
    way_of = (codes >= tokens).astype(jnp.int32)
    spot_of = jnp.where(
        way_of == 1, rows + base[1][:, None] + codes - tokens, base[0][:, None] + codes
    )
    spot_of = jnp.where(codes >= 2 * tokens, 2 * rows + codes - 2 * tokens, spot_of)
    expert = jnp.clip(jnp.where(codes >= 0, spot_of, zero_row), 0, zero_row).reshape(-1)

    total = ep * capacity
    index = jnp.arange(total, dtype=jnp.int32) + 1
    here = (expert[:, None] // CHUNK == jnp.arange(2 * CHUNKS, dtype=jnp.int32)[None]).astype(
        jnp.bfloat16
    )
    inner = expert[:, None] % CHUNK == jnp.arange(CHUNK, dtype=jnp.int32)[None]
    parts = [
        jnp.where(inner, part[:, None], 0).astype(jnp.bfloat16)
        for part in (index // LANES, index % LANES)
    ]
    found = lax.dot_general(
        here,
        jnp.concatenate(parts, axis=1),
        (((0,), (0,)), ((), ())),
        preferred_element_type=jnp.float32,
    ).astype(jnp.int32)
    found = (found[:, :CHUNK] * LANES + found[:, CHUNK:]).reshape(2, rows)
    first_result = none_row + CHUNK
    result_pick = jnp.where(found > 0, first_result + found - 1, none_row)

    back = jnp.where(reach > 0, way_base + rank, none_row)
    mine = route_ids == me
    local = jnp.sum(jnp.where(mine, first_result + target - none_row, 0), axis=1) + none_row
    final = jnp.concatenate([jnp.clip(back, 0, none_row), local[None]], axis=0)
    return fits, pick, expert, result_pick, onward, final


def feed_forward(rows, full_gate, full_up, full_down):
    gate_pre = jnp.dot(rows, full_gate, preferred_element_type=jnp.float32)
    up_pre = jnp.dot(rows, full_up, preferred_element_type=jnp.float32)
    hidden = (jax.nn.silu(gate_pre) * up_pre).astype(jnp.bfloat16)
    return jnp.dot(hidden, full_down, preferred_element_type=jnp.float32).astype(jnp.bfloat16)


def padded_exchange(normed, target, route_weights, weights, ep_size, capacity):
    row_count, features = normed.shape
    outbound = jnp.zeros((ep_size * capacity, features), jnp.bfloat16)
    for column in range(target.shape[1]):
        outbound = outbound.at[target[:, column]].set(normed)
    outbound = outbound.reshape(ep_size, capacity, features)
    arrived = lax.all_to_all(outbound, "ep", split_axis=0, concat_axis=0, tiled=True)
    result = feed_forward(arrived.reshape(-1, features), *weights)
    returned_rows = send_back(result.reshape(ep_size, capacity, features))
    returned_rows = returned_rows.reshape(ep_size * capacity, features)
    combined = jnp.zeros((row_count, features), jnp.float32)
    for column in range(target.shape[1]):
        picked = returned_rows[target[:, column]].astype(jnp.float32)
        combined = combined + route_weights[:, column : column + 1] * picked
    return combined.astype(jnp.bfloat16)


def per_device(
    tokens,
    norm_gain,
    route_ids,
    route_weights,
    w_gate,
    w_up,
    w_down,
    dispatch=dispatch,
    collect=collect,
    starts_of=stream_starts,
):
    row_count, features = tokens.shape
    ep_size = lax.axis_size("ep")
    capacity = row_count * GROUPS // ep_size
    floats = tokens.astype(jnp.float32)
    inverse = lax.rsqrt(jnp.mean(floats * floats, axis=1, keepdims=True) + epsilon)
    normed = (floats * inverse * norm_gain).astype(jnp.bfloat16)
    message, reach, rank, target, steps = plan_routes(route_ids, route_weights, capacity)
    arrived = lax.all_to_all(message, "ep", split_axis=0, concat_axis=0, tiled=True)
    fits, pick, expert, result_pick, onward, final = plan_streams(
        arrived, reach, rank, target, route_ids, steps, capacity, starts_of
    )
    expert_rows, *weights = dispatch(
        pick, expert, normed.reshape(row_count, -1, LANES), (w_gate[0], w_up[0], w_down[0])
    )
    result = feed_forward(expert_rows.reshape(-1, features), *weights)
    scale = arrived[:, capacity : 2 * capacity].reshape(-1, 1)
    result = (result.astype(jnp.float32) * scale).astype(jnp.bfloat16)
    result = result.reshape(-1, features // LANES, LANES)
    mixed = collect(result_pick, onward, final, result).reshape(row_count, features)
    return lax.cond(
        fits,
        lambda: mixed,
        lambda: padded_exchange(normed, target, route_weights, weights, ep_size, capacity),
    )


def solution(mesh):
    in_specs = (
        P(("grp", "ep", "tp"), None),
        P(),
        P(("grp", "ep", "tp"), None),
        P(("grp", "ep", "tp"), None),
        P("ep", None, "tp"),
        P("ep", None, "tp"),
        P("ep", "tp", None),
    )
    out_specs = P(("grp", "ep", "tp"), None)
    return jax.shard_map(
        per_device, mesh=mesh, in_specs=in_specs, out_specs=out_specs, check_vma=False
    )
```

profile of v0, /device:TPU:46, one launch (start us, length us, event | category | flops | bytes accessed | tf_op | source)
XLA Modules:
  0.0 479.2 jit_solution(14932788722693599997)
XLA Ops:
  0.1 0.8 fusion.78
  0.8 1.0 convert_reduce_fusion.1
  1.8 0.7 select_reduce_fusion.15
  2.6 0.2 fusion.34
  2.8 0.7 fusion.69
  3.5 1.3 fusion.62
  4.8 0.6 broadcast_compare_fusion.1
  5.4 0.6 reshape_select_fusion.1
  6.0 0.6 reshape_select_fusion
  6.6 0.3 convert_reduce_fusion
  6.9 0.1 convert_reduce_fusion.3
  7.0 0.7 fusion.45
  7.7 0.8 fusion.75
  8.5 0.4 select_reduce_fusion.2
  8.9 0.4 select_reduce_fusion.3
  9.7 0.6 pad.11
  10.3 32.7 %all-to-all-start.2 = ((f32[32,1,128]{2,1,0:T(1,128)}), f32[32,1,128]{2,1,0:T(1,128)S(1)}, u32[]{:S(2)}, u32[]{:S(2)}) async-start(f32[32,1,128]{2,1,0:T(1,128)} %bitcast.22), calls=%async_computation.2 | async-start | bytes 32768 | tf_op jit(solution)/shard_map/all_to_all | solution.py:519
  43.0 1.5 fusion.10
  44.6 1.0 fusion.89
  45.6 0.3 fusion.12
  46.2 0.6 pad_add_fusion.final_ref
  46.8 1.2 copy.52
  48.0 0.1 select_reduce_fusion.4
  48.2 16.4 %all-to-all-done.2 = f32[32,1,128]{2,1,0:T(1,128)S(1)} async-done(((f32[32,1,128]{2,1,0:T(1,128)}), f32[32,1,128]{2,1,0:T(1,128)S(1)}, u32[]{:S(2)}, u32[]{:S(2)}) %all-to-all-start.2) | async-done | bytes 16416 | tf_op jit(solution)/shard_map/all_to_all | solution.py:519
  64.6 0.7 copy.39.counts_ref
  65.3 3.0 starts.1
  68.3 1.5 fusion.30
  70.5 0.3 fusion.21
  70.9 0.1 copy.48
  71.0 0.3 fusion.22
  71.3 0.1 copy.49
  71.4 0.1 copy.50
  71.7 0.2 iota_compare_fusion.8
  71.9 0.1 select_reduce_fusion.14
  72.3 0.6 select_reduce_fusion.11
  72.9 0.9 select_reduce_fusion.8
  73.8 0.7 fusion.37
  74.5 191.1 %dispatch.1 = (bf16[1024,16,128]{2,1,0:T(8,128)(2,1)}, bf16[2048,512]{1,0:T(8,128)(2,1)}, bf16[2048,512]{1,0:T(8,128)(2,1)}, bf16[512,2048]{1,0:T(8,128)(2,1)}) custom-call(s32[2,1856]{1,0:T(2,128)} %get-tuple-element.97.pick_ref, s32[1024]{0:T(1024)} %copy-done.3, bf16[256,16,128]{2,1,0:T(8,128)(2,1)} %bitcast.89, bf16[2048,256]{1,0:T(8,128)(2,1)} %bitcast.90, ...), custom_call_target="tpu_custom_call" | custom-call | tf_op jit(solution)/shard_map/dispatch/pallas_call | solution.py:255
  265.6 6.5 %fusion.6 = f32[1024,512]{1,0:T(8,128)} fusion(bf16[2048,512]{1,0:T(8,128)(2,1)} %get-tuple-element.37, bf16[128,8,16,128]{3,2,1,0:T(8,128)(2,1)} %bitcast.121), kind=kOutput, calls=%fused_computation.19 | convolution fusion | flops 2147483648 | bytes 8388608 | tf_op jit(solution)/shard_map/dot_general | solution.py:477
  272.2 10.6 %fusion.3 = bf16[128,8,16,128]{3,1,2,0:T(8,128)(2,1)} fusion(f32[1024]{0:T(1024)S(1)} %mul.115, bf16[512,2048]{1,0:T(8,128)(2,1)} %get-tuple-element.39, f32[1024,512]{1,0:T(8,128)} %fusion.6, bf16[2048,512]{1,0:T(8,128)(2,1)} %get-tuple-element.38, bf16[128,8,16,128]{3,2,1,0:T(8,128)(2,1)} %bitcast.122), kind=kOutput, calls=%fused_computation.16 | convolution fusion | flops 4306501632 | bytes 14684160 | tf_op jit(solution)/shard_map/dot_general | solution.py:480
  282.8 5.5 %copy.54 = bf16[128,8,16,128]{3,2,1,0:T(8,128)(2,1)} copy(bf16[128,8,16,128]{3,1,2,0:T(8,128)(2,1)} %fusion.3) | data formatting | bytes 8388608
  288.3 0.5 fusion.16
  288.9 0.1 copy.43
  289.0 0.8 select_n.414.result_ref
  290.4 187.3 %collect.1 = bf16[256,16,128]{2,1,0:T(8,128)(2,1)S(1)} custom-call(s32[2,1856]{1,0:T(2,128)} %select_n.414.result_ref, s32[2,1856]{1,0:T(2,128)} %get-tuple-element.96.onward_ref, s32[3,256]{1,0:T(4,128)} %pad_add_fusion.final_ref, bf16[1024,16,128]{2,1,0:T(8,128)(2,1)} %bitcast.84), custom_call_target="tpu_custom_call" | custom-call | tf_op jit(solution)/shard_map/collect/pallas_call | solution.py:269
  477.7 0.6 conditional.1
  477.9 0.3 copy.68
  478.2 1.0 copy-done.2
  (62 shorter events, 2.3 us)
Async XLA Ops:
  0.0 44.5 %copy-start = (bf16[256,2048]{1,0:T(8,128)(2,1)S(1)}, bf16[256,2048]{1,0:T(8,128)(2,1)}, u32[]{:S(2)}) copy-start(bf16[256,2048]{1,0:T(8,128)(2,1)} %param.9) | copy-start | bytes 3145732
  0.0 45.6 %copy-start.4 = (f32[2048]{0:T(1024)S(1)}, f32[2048]{0:T(1024)}, u32[]{:S(2)}) copy-start(f32[2048]{0:T(1024)} %param.10) | copy-start | bytes 24580
  10.3 54.3 %all-to-all-start.2 = ((f32[32,1,128]{2,1,0:T(1,128)}), f32[32,1,128]{2,1,0:T(1,128)S(1)}, u32[]{:S(2)}, u32[]{:S(2)}) async-start(f32[32,1,128]{2,1,0:T(1,128)} %bitcast.22), calls=%async_computation.2 | async-start | bytes 32768 | tf_op jit(solution)/shard_map/all_to_all | solution.py:519
  72.2 2.3 copy-start.3
  282.8 7.6 %copy-start.5 = (f32[256,2]{0,1:T(2,128)S(1)}, f32[256,2]{0,1:T(2,128)}, u32[]{:S(2)}) copy-start(f32[256,2]{0,1:T(2,128)} %param.12) | copy-start | bytes 6148
  478.2 1.0 copy-start.2
where the time goes:
time: 480 us; the launch traced here: 479 us
  Pallas kernels  381 us (79%)
  starting transfers between devices  32.7 us (7%)
  matrix products  17.7 us (4%)
  other arithmetic  16.5 us (3%)
  waiting for transfers between devices  16.4 us (3%)
  local copies, waits for them, and re-layouts  13.4 us (3%)
    pallas_call x1, Pallas kernels, dispatch(): pl.pallas_call(dispatch_kernel, out_shape=[jax.ShapeDtypeStruct((expert.s...  191 us
    pallas_call x1, Pallas kernels, collect(): pl.pallas_call(collect_kernel, out_shape=jax.ShapeDtypeStruct((final.shap...  187 us
    all_to_all x1, starting transfers between devices, per_device(): lax.all_to_all(message, 'ep', split_axis=0, concat_axis=0, tiled=True)  32.7 us
    all_to_all x1, waiting for transfers between devices, per_device(): lax.all_to_all(message, 'ep', split_axis=0, concat_axis=0, tiled=True)  16.4 us
    dot_general x1, matrix products, feed_forward(): jnp.dot(hidden, full_down, preferred_element_type=jnp.float32)  10.6 us
  transfers between devices with their start and end apart: 1, of which 1 were waited for; matrix products, arithmetic and copies ran while one was open for 1% of the time, Pallas kernels for 0%

commit v1 on v0

--- a/solution.py
+++ b/solution.py
@@ -12,8 +12,8 @@
 epsilon = 1e-06
 
 CHUNK = 8
-LAG = 5
-CHUNKS = 232
+LAG = 6
+CHUNKS = 238
 BIAS = 6
 SLOTS = 8
 LANES = 128
@@ -90,10 +90,11 @@
 
 def half_copies(halves, wholes, half_sem, own_sem, half, other):
     remote, local = [], []
-    for index, (part, whole) in enumerate(zip(halves, wholes)):
+    for index, (part, whole, group) in enumerate(zip(halves, wholes, (0, 1, 0))):
         if part.shape[0] == whole.shape[0]:
             width = part.shape[1]
-            place = whole.at[:, pl.ds(pl.multiple_of(half * width, width), width)]
+            at = (2 * group + half) * width
+            place = whole.at[:, pl.ds(pl.multiple_of(at, width), width)]
         else:
             depth = part.shape[0]
             place = whole.at[pl.ds(pl.multiple_of(half * depth, depth), depth)]
@@ -119,8 +120,7 @@
     up_half,
     down_half,
     out_ref,
-    gate_whole,
-    up_whole,
+    gate_up_whole,
     down_whole,
     store,
     send,
@@ -135,7 +135,7 @@
     other = {"tp": 1 - half}
     peers = ring_setup([other])
     halves = (gate_half, up_half, down_half)
-    wholes = (gate_whole, up_whole, down_whole)
+    wholes = (gate_up_whole, gate_up_whole, down_whole)
     remote, local = half_copies(halves, wholes, half_sem, own_sem, half, other)
     for copy in remote + local:
         copy.start()
@@ -247,16 +247,16 @@
 
 def dispatch(pick, expert, own, halves):
     row_shape = own.shape[1:]
-    gate_half, up_half, down_half = halves
+    gate_half, _, down_half = halves
     wholes = [
-        jax.ShapeDtypeStruct((part.shape[0], part.shape[1] * 2), part.dtype)
-        for part in (gate_half, up_half)
-    ] + [jax.ShapeDtypeStruct((down_half.shape[0] * 2, down_half.shape[1]), down_half.dtype)]
+        jax.ShapeDtypeStruct((gate_half.shape[0], 4 * gate_half.shape[1]), gate_half.dtype),
+        jax.ShapeDtypeStruct((down_half.shape[0] * 2, down_half.shape[1]), down_half.dtype),
+    ]
     return pl.pallas_call(
         dispatch_kernel,
         out_shape=[jax.ShapeDtypeStruct((expert.shape[0],) + row_shape, jnp.bfloat16)] + wholes,
         in_specs=[SMEM, SMEM, VMEM, ANY, ANY, ANY],
-        out_specs=[VMEM, ANY, ANY, ANY],
+        out_specs=[VMEM, ANY, ANY],
         scratch_shapes=ring_scratch(2 * CHUNKS * CHUNK + own.shape[0] + 1, row_shape)
         + [pltpu.SemaphoreType.DMA((2, 3)), pltpu.SemaphoreType.DMA((3,))],
         compiler_params=ring_params(0),
@@ -473,21 +473,25 @@
     return fits, pick, expert, result_pick, onward, final
 
 
-def feed_forward(rows, full_gate, full_up, full_down):
-    gate_pre = jnp.dot(rows, full_gate, preferred_element_type=jnp.float32)
-    up_pre = jnp.dot(rows, full_up, preferred_element_type=jnp.float32)
+def feed_forward(rows, gate_up, full_down):
+    both = jnp.dot(rows, gate_up, preferred_element_type=jnp.float32)
+    gate_pre, up_pre = jnp.split(both, 2, axis=1)
     hidden = (jax.nn.silu(gate_pre) * up_pre).astype(jnp.bfloat16)
     return jnp.dot(hidden, full_down, preferred_element_type=jnp.float32).astype(jnp.bfloat16)
 
 
 def padded_exchange(normed, target, route_weights, weights, ep_size, capacity):
     row_count, features = normed.shape
-    outbound = jnp.zeros((ep_size * capacity, features), jnp.bfloat16)
-    for column in range(target.shape[1]):
-        outbound = outbound.at[target[:, column]].set(normed)
+    slots = jnp.arange(ep_size * capacity, dtype=jnp.int32)
+    chosen = (slots[:, None] == target[None, :, 0]) | (slots[:, None] == target[None, :, 1])
+    outbound = jnp.dot(
+        chosen.astype(jnp.bfloat16), normed, preferred_element_type=jnp.float32
+    ).astype(jnp.bfloat16)
     outbound = outbound.reshape(ep_size, capacity, features)
     arrived = lax.all_to_all(outbound, "ep", split_axis=0, concat_axis=0, tiled=True)
-    result = feed_forward(arrived.reshape(-1, features), *weights)
+    result = lax.map(
+        lambda rows: feed_forward(rows, *weights), arrived.reshape(-1, 128, features)
+    )
     returned_rows = send_back(result.reshape(ep_size, capacity, features))
     returned_rows = returned_rows.reshape(ep_size * capacity, features)
     combined = jnp.zeros((row_count, features), jnp.float32)

time: 480 us -> 451 us (0.940)
  Pallas kernels: 381 us -> 362 us
  matrix products: 17.7 us -> 10.7 us
    pallas_call x1, Pallas kernels: 191 us -> 180 us  [dispatch(): pl.pallas_call(dispatch_kernel, out_shape=[jax.ShapeDtypeStruct((expert.s...]
    pallas_call x1, Pallas kernels: 187 us -> 179 us  [collect(): pl.pallas_call(collect_kernel, out_shape=jax.ShapeDtypeStruct((final.shap...]
    dot_general x1, matrix products: 10.6 us -> 2.5 us  [feed_forward(): jnp.dot(hidden, full_down, preferred_element_type=jnp.float32)]
where the time goes in v1:
time: 451 us
  Pallas kernels  362 us (80%)
  starting transfers between devices  32.8 us (7%)
  other arithmetic  17.7 us (4%)
  waiting for transfers between devices  14.9 us (3%)
  local copies, waits for them, and re-layouts  11.3 us (3%)
  matrix products  10.7 us (2%)
    pallas_call x1, Pallas kernels, dispatch(): pl.pallas_call(dispatch_kernel, out_shape=[jax.ShapeDtypeStruct((expert.s...  180 us
    pallas_call x1, Pallas kernels, collect(): pl.pallas_call(collect_kernel, out_shape=jax.ShapeDtypeStruct((final.shap...  179 us
    all_to_all x1, starting transfers between devices, per_device(): lax.all_to_all(message, 'ep', split_axis=0, concat_axis=0, tiled=True)  32.8 us
    all_to_all x1, waiting for transfers between devices, per_device(): lax.all_to_all(message, 'ep', split_axis=0, concat_axis=0, tiled=True)  14.9 us
  transfers between devices with their start and end apart: 1, of which 1 were waited for; matrix products, arithmetic and copies ran while one was open for 1% of the time, Pallas kernels for 0%

profile of v1, /device:TPU:46, one launch (start us, length us, event | category | flops | bytes accessed | tf_op | source)
XLA Modules:
  0.0 450.6 jit_solution(562092751918373708)
XLA Ops:
  0.1 0.8 fusion.84
  0.8 1.0 convert_reduce_fusion.1
  1.8 0.7 select_reduce_fusion.15
  2.6 0.2 fusion.40
  2.8 0.7 fusion.75
  3.5 1.3 fusion.68
  4.8 0.6 broadcast_compare_fusion.1
  5.4 0.6 reshape_select_fusion.1
  6.0 0.6 reshape_select_fusion
  6.6 0.3 convert_reduce_fusion
  6.9 0.1 convert_reduce_fusion.3
  7.0 0.7 fusion.51
  7.7 0.8 fusion.81
  8.5 0.4 select_reduce_fusion.2
  8.9 0.4 select_reduce_fusion.3
  9.7 0.6 pad.11
  10.3 32.8 %all-to-all-start.2 = ((f32[32,1,128]{2,1,0:T(1,128)}), f32[32,1,128]{2,1,0:T(1,128)S(1)}, u32[]{:S(2)}, u32[]{:S(2)}) async-start(f32[32,1,128]{2,1,0:T(1,128)} %bitcast.26), calls=%async_computation.2 | async-start | bytes 32768 | tf_op jit(solution)/shard_map/all_to_all | solution.py:523
  43.2 1.5 fusion.18
  44.7 1.6 fusion.91
  46.3 1.0 fusion.20
  47.6 0.6 pad_add_fusion.final_ref
  48.3 1.2 copy.52
  49.5 0.1 select_reduce_fusion.4
  49.6 14.9 %all-to-all-done.2 = f32[32,1,128]{2,1,0:T(1,128)S(1)} async-done(((f32[32,1,128]{2,1,0:T(1,128)}), f32[32,1,128]{2,1,0:T(1,128)S(1)}, u32[]{:S(2)}, u32[]{:S(2)}) %all-to-all-start.2) | async-done | bytes 16416 | tf_op jit(solution)/shard_map/all_to_all | solution.py:523
  64.6 0.7 copy.39.counts_ref
  65.3 3.0 starts.1
  68.3 1.4 fusion.36
  70.4 0.3 fusion.27
  70.8 0.1 copy.48
  70.9 0.3 fusion.28
  71.2 0.1 copy.49
  71.3 0.1 copy.50
  71.6 0.2 iota_compare_fusion.11
  71.8 0.1 select_reduce_fusion.14
  72.2 0.6 select_reduce_fusion.11
  72.8 0.9 select_reduce_fusion.8
  73.7 0.7 fusion.43
  74.5 180.4 %dispatch.1 = (bf16[1024,16,128]{2,1,0:T(8,128)(2,1)}, bf16[2048,1024]{1,0:T(8,128)(2,1)}, bf16[512,2048]{1,0:T(8,128)(2,1)}) custom-call(s32[2,1904]{1,0:T(2,128)} %get-tuple-element.131.pick_ref, s32[1024]{0:T(1024)} %copy-done.2, bf16[256,16,128]{2,1,0:T(8,128)(2,1)} %bitcast.94, bf16[2048,256]{1,0:T(8,128)(2,1)} %bitcast.95, bf16[2048,256]{1,0:T(8,128)(2,1)} %bitcast.96, ...), custom_call_target="tpu_custom_call" | custom-call | tf_op jit(solution)/shard_map/dispatch/pallas_call | solution.py:255
  254.9 7.7 %fusion.15 = f32[1024,1024]{1,0:T(8,128)S(1)} fusion(bf16[2048,1024]{1,0:T(8,128)(2,1)} %get-tuple-element.60, bf16[128,8,16,128]{3,2,1,0:T(8,128)(2,1)} %bitcast.126), kind=kOutput, calls=%fused_computation.27 | convolution fusion | flops 4294967296 | bytes 12582912 | tf_op jit(solution)/shard_map/dot_general | solution.py:477
  262.5 2.5 fusion.14
  265.1 3.4 copy.54
  268.4 0.5 fusion.23
  269.0 0.1 copy.43
  269.1 0.8 select_n.412.result_ref
  270.4 178.9 %collect.1 = bf16[256,16,128]{2,1,0:T(8,128)(2,1)S(1)} custom-call(s32[2,1904]{1,0:T(2,128)} %select_n.412.result_ref, s32[2,1904]{1,0:T(2,128)} %get-tuple-element.130.onward_ref, s32[3,256]{1,0:T(4,128)} %pad_add_fusion.final_ref, bf16[1024,16,128]{2,1,0:T(8,128)(2,1)} %bitcast.92), custom_call_target="tpu_custom_call" | custom-call | tf_op jit(solution)/shard_map/collect/pallas_call | solution.py:269
  449.3 0.3 conditional.1
  449.3 0.3 copy.60
  449.6 1.0 copy-done.1
  (62 shorter events, 2.3 us)
Async XLA Ops:
  0.0 46.3 %copy-start = (bf16[256,2048]{1,0:T(8,128)(2,1)S(1)}, bf16[256,2048]{1,0:T(8,128)(2,1)}, u32[]{:S(2)}) copy-start(bf16[256,2048]{1,0:T(8,128)(2,1)} %param.11) | copy-start | bytes 3145732
  10.3 54.3 %all-to-all-start.2 = ((f32[32,1,128]{2,1,0:T(1,128)}), f32[32,1,128]{2,1,0:T(1,128)S(1)}, u32[]{:S(2)}, u32[]{:S(2)}) async-start(f32[32,1,128]{2,1,0:T(1,128)} %bitcast.26), calls=%async_computation.2 | async-start | bytes 32768 | tf_op jit(solution)/shard_map/all_to_all | solution.py:523
  72.1 2.3 copy-start.2
  254.8 7.7 %copy-start.4 = (bf16[512,2048]{1,0:T(8,128)(2,1)S(1)}, bf16[512,2048]{1,0:T(8,128)(2,1)}, u32[]{:S(2)}) copy-start(bf16[512,2048]{1,0:T(8,128)(2,1)} %get-tuple-element.61) | copy-start | bytes 6291460
  265.0 5.4 %copy-start.3 = (f32[256,2]{0,1:T(2,128)S(1)}, f32[256,2]{0,1:T(2,128)}, u32[]{:S(2)}) copy-start(f32[256,2]{0,1:T(2,128)} %param.14) | copy-start | bytes 6148
  449.6 1.0 copy-start.1

commit v2 on v1

--- a/solution.py
+++ b/solution.py
@@ -49,11 +49,10 @@
 
 
 def ring_stream(peers, order, build, keep, send, land, send_sem, recv_sem):
-    def receive(step):
-        for way in (0, 1):
-            chunk = order(step)
-            chunk_copy(send, land, send_sem, recv_sem, peers[way], way, 0, chunk).wait_recv()
-            keep(way, chunk)
+    def receive(way, step):
+        chunk = order(step)
+        chunk_copy(send, land, send_sem, recv_sem, peers[way], way, 0, chunk).wait_recv()
+        keep(way, chunk)
 
     def drain(step):
         slot = lax.rem(step, SLOTS)
@@ -65,15 +64,16 @@
     def body(step, carry):
         slot = lax.rem(step, SLOTS)
 
-        @pl.when(step >= LAG)
-        def _():
-            receive(step - LAG)
-
         @pl.when(step >= SLOTS)
         def _():
             drain(step - SLOTS)
 
         for way in (0, 1):
+
+            @pl.when(step >= LAG)
+            def _():
+                receive(way, step - LAG)
+
             build(way, slot, order(step))
         for way in (0, 1):
             chunk_copy(
@@ -83,7 +83,8 @@
 
     lax.fori_loop(0, CHUNKS, body, 0)
     for step in range(CHUNKS - LAG, CHUNKS):
-        receive(step)
+        for way in (0, 1):
+            receive(way, step)
     for step in range(CHUNKS - SLOTS, CHUNKS):
         drain(step)
 
@@ -129,8 +130,12 @@
     recv_sem,
     half_sem,
     own_sem,
+    load_sem,
 ):
     rows = CHUNKS * CHUNK
+    own_rows = own_ref.shape[0]
+    load = pltpu.make_async_copy(own_ref, store.at[pl.ds(2 * rows, own_rows)], load_sem)
+    load.start()
     half = lax.axis_index("tp")
     other = {"tp": 1 - half}
     peers = ring_setup([other])
@@ -139,32 +144,28 @@
     remote, local = half_copies(halves, wholes, half_sem, own_sem, half, other)
     for copy in remote + local:
         copy.start()
-    own_rows = own_ref.shape[0]
-
-    def take(block, carry):
-        at = pl.multiple_of(block * CHUNK, CHUNK)
-        store[pl.ds(2 * rows + at, CHUNK)] = own_ref[pl.ds(at, CHUNK)]
-        return carry
-
-    lax.fori_loop(0, own_rows // CHUNK, take, 0)
     store[pl.ds(2 * rows + own_rows, 1)] = jnp.zeros((1,) + own_ref.shape[1:], own_ref.dtype)
+    load.wait()
 
     def keep(way, chunk):
         store[pl.ds(way * rows + chunk * CHUNK, CHUNK)] = land[way, chunk]
 
     def build(way, slot, chunk):
-        for row in range(CHUNK):
-            send[way, slot, row] = store[pick_ref[way, chunk * CHUNK + row]]
+        taken = [store[pick_ref[way, chunk * CHUNK + row]] for row in range(CHUNK)]
+        for row, value in enumerate(taken):
+            send[way, slot, row] = value
 
     ring_stream(peers, lambda step: step, build, keep, send, land, send_sem, recv_sem)
 
+    batch = 2 * CHUNK
+
     def gather(block, carry):
-        for row in range(CHUNK):
-            at = block * CHUNK + row
-            out_ref[at] = store[expert_ref[at]]
+        taken = [store[expert_ref[block * batch + row]] for row in range(batch)]
+        for row, value in enumerate(taken):
+            out_ref[block * batch + row] = value
         return carry
 
-    lax.fori_loop(0, out_ref.shape[0] // CHUNK, gather, 0)
+    lax.fori_loop(0, out_ref.shape[0] // batch, gather, 0)
     for copy in remote + local:
         copy.wait()
 
@@ -195,11 +196,11 @@
         store[pl.ds(way * rows + chunk * CHUNK, CHUNK)] = land[way, chunk]
 
     def build(way, slot, chunk):
-        for row in range(CHUNK):
-            at = chunk * CHUNK + row
-            here = store[result_ref[way, at]].astype(jnp.float32)
-            beyond = store[onward_ref[way, at]].astype(jnp.float32)
-            send[way, slot, row] = (here + beyond).astype(send.dtype)
+        places = [chunk * CHUNK + row for row in range(CHUNK)]
+        pairs = [(store[result_ref[way, at]], store[onward_ref[way, at]]) for at in places]
+        for row, (here, beyond) in enumerate(pairs):
+            total = here.astype(jnp.float32) + beyond.astype(jnp.float32)
+            send[way, slot, row] = total.astype(send.dtype)
 
     ring_stream(
         (down, up),
@@ -213,11 +214,11 @@
     )
 
     def finish(block, carry):
-        for row in range(CHUNK):
-            at = block * CHUNK + row
-            total = store[final_ref[2, at]].astype(jnp.float32)
-            for way in (0, 1):
-                total = total + store[final_ref[way, at]].astype(jnp.float32)
+        places = [block * CHUNK + row for row in range(CHUNK)]
+        parts = [[store[final_ref[index, at]] for index in (2, 0, 1)] for at in places]
+        for at, (local, above, below) in zip(places, parts):
+            total = local.astype(jnp.float32) + above.astype(jnp.float32)
+            total = total + below.astype(jnp.float32)
             out_ref[at] = total.astype(out_ref.dtype)
         return carry
 
@@ -255,10 +256,14 @@
     return pl.pallas_call(
         dispatch_kernel,
         out_shape=[jax.ShapeDtypeStruct((expert.shape[0],) + row_shape, jnp.bfloat16)] + wholes,
-        in_specs=[SMEM, SMEM, VMEM, ANY, ANY, ANY],
+        in_specs=[SMEM, SMEM, ANY, ANY, ANY, ANY],
         out_specs=[VMEM, ANY, ANY],
         scratch_shapes=ring_scratch(2 * CHUNKS * CHUNK + own.shape[0] + 1, row_shape)
-        + [pltpu.SemaphoreType.DMA((2, 3)), pltpu.SemaphoreType.DMA((3,))],
+        + [
+            pltpu.SemaphoreType.DMA((2, 3)),
+            pltpu.SemaphoreType.DMA((3,)),
+            pltpu.SemaphoreType.DMA,
+        ],
         compiler_params=ring_params(0),
         name="dispatch",
     )(pick, expert, own, *halves)
@@ -279,18 +284,22 @@
 
 
 def starts_kernel(steps, counts_ref, starts_ref, lives_ref):
-    for way, shift in ((0, 1), (1, LANES - 1)):
-        start = jnp.zeros((1, LANES), jnp.int32)
-        live = counts_ref[way * steps : way * steps + 1]
-        for distance in range(steps):
+    shifts = (1, LANES - 1)
+    start = [jnp.zeros((1, LANES), jnp.int32)] * 2
+    live = [None, None]
+    for distance in range(steps):
+        for way in (0, 1):
+            at = way * steps + distance
             if distance:
-                start = jnp.maximum(
-                    start + live, pltpu.roll(start, shift, axis=1) + LAG * CHUNK
+                start[way] = jnp.maximum(
+                    start[way] + live[way],
+                    pltpu.roll(start[way], shifts[way], axis=1) + LAG * CHUNK,
                 )
-                at = way * steps + distance
-                live = pltpu.roll(counts_ref[at : at + 1], shift * distance % LANES, axis=1)
-            starts_ref[way * steps + distance : way * steps + distance + 1] = start
-            lives_ref[way * steps + distance : way * steps + distance + 1] = live
+            live[way] = counts_ref[at : at + 1]
+            if distance:
+                live[way] = pltpu.roll(live[way], shifts[way] * distance % LANES, axis=1)
+            starts_ref[at : at + 1] = start[way]
+            lives_ref[at : at + 1] = live[way]
 
 
 def stream_starts(counts, steps):

time: 451 us -> 451 us (level)
  no operation moved by 1% of the time
where the time goes in v2:
time: 451 us; the launch traced here: 450 us
  Pallas kernels  362 us (80%)
  starting transfers between devices  32.8 us (7%)
  other arithmetic  17.7 us (4%)
  waiting for transfers between devices  14.9 us (3%)
  local copies, waits for them, and re-layouts  11.3 us (3%)
  matrix products  10.7 us (2%)
    pallas_call x1, Pallas kernels, dispatch(): pl.pallas_call(dispatch_kernel, out_shape=[jax.ShapeDtypeStruct((expert.s...  180 us
    pallas_call x1, Pallas kernels, collect(): pl.pallas_call(collect_kernel, out_shape=jax.ShapeDtypeStruct((final.shap...  179 us
    all_to_all x1, starting transfers between devices, per_device(): lax.all_to_all(message, 'ep', split_axis=0, concat_axis=0, tiled=True)  32.8 us
    all_to_all x1, waiting for transfers between devices, per_device(): lax.all_to_all(message, 'ep', split_axis=0, concat_axis=0, tiled=True)  14.9 us
  transfers between devices with their start and end apart: 1, of which 1 were waited for; matrix products, arithmetic and copies ran while one was open for 1% of the time, Pallas kernels for 0%

profile of v2, /device:TPU:46, one launch (start us, length us, event | category | flops | bytes accessed | tf_op | source)
XLA Modules:
  0.0 450.3 jit_solution(6979759414861915478)
XLA Ops:
  0.1 0.8 fusion.84
  0.8 1.0 convert_reduce_fusion.1
  1.8 0.7 select_reduce_fusion.15
  2.6 0.2 fusion.40
  2.8 0.7 fusion.75
  3.5 1.3 fusion.68
  4.8 0.6 broadcast_compare_fusion.1
  5.4 0.6 reshape_select_fusion.1
  6.0 0.6 reshape_select_fusion
  6.6 0.3 convert_reduce_fusion
  6.9 0.1 convert_reduce_fusion.3
  7.0 0.7 fusion.51
  7.7 0.8 fusion.81
  8.5 0.4 select_reduce_fusion.2
  8.9 0.4 select_reduce_fusion.3
  9.7 0.6 pad.11
  10.3 32.8 %all-to-all-start.2 = ((f32[32,1,128]{2,1,0:T(1,128)}), f32[32,1,128]{2,1,0:T(1,128)S(1)}, u32[]{:S(2)}, u32[]{:S(2)}) async-start(f32[32,1,128]{2,1,0:T(1,128)} %bitcast.26), calls=%async_computation.2 | async-start | bytes 32768 | tf_op jit(solution)/shard_map/all_to_all | solution.py:532
  43.2 1.5 fusion.18
  44.7 1.6 fusion.91
  46.3 1.0 fusion.20
  47.6 0.6 pad_add_fusion.final_ref
  48.3 1.2 copy.52
  49.5 0.1 select_reduce_fusion.4
  49.6 14.9 %all-to-all-done.2 = f32[32,1,128]{2,1,0:T(1,128)S(1)} async-done(((f32[32,1,128]{2,1,0:T(1,128)}), f32[32,1,128]{2,1,0:T(1,128)S(1)}, u32[]{:S(2)}, u32[]{:S(2)}) %all-to-all-start.2) | async-done | bytes 16416 | tf_op jit(solution)/shard_map/all_to_all | solution.py:532
  64.6 0.7 copy.39.counts_ref
  65.3 3.0 starts.1
  68.3 1.4 fusion.36
  70.4 0.3 fusion.27
  70.8 0.1 copy.48
  70.9 0.3 fusion.28
  71.2 0.1 copy.49
  71.3 0.1 copy.50
  71.6 0.2 iota_compare_fusion.11
  71.8 0.1 select_reduce_fusion.14
  72.2 0.6 select_reduce_fusion.11
  72.8 0.9 select_reduce_fusion.8
  73.7 0.7 fusion.43
  74.5 179.7 %dispatch.1 = (bf16[1024,16,128]{2,1,0:T(8,128)(2,1)}, bf16[2048,1024]{1,0:T(8,128)(2,1)}, bf16[512,2048]{1,0:T(8,128)(2,1)}) custom-call(s32[2,1904]{1,0:T(2,128)} %get-tuple-element.131.pick_ref, s32[1024]{0:T(1024)} %copy-done.2, bf16[256,16,128]{2,1,0:T(8,128)(2,1)} %bitcast.94, bf16[2048,256]{1,0:T(8,128)(2,1)} %bitcast.95, bf16[2048,256]{1,0:T(8,128)(2,1)} %bitcast.96, ...), custom_call_target="tpu_custom_call" | custom-call | tf_op jit(solution)/shard_map/dispatch/pallas_call | solution.py:256
  254.2 7.7 %fusion.15 = f32[1024,1024]{1,0:T(8,128)S(1)} fusion(bf16[2048,1024]{1,0:T(8,128)(2,1)} %get-tuple-element.60, bf16[128,8,16,128]{3,2,1,0:T(8,128)(2,1)} %bitcast.126), kind=kOutput, calls=%fused_computation.27 | convolution fusion | flops 4294967296 | bytes 12582912 | tf_op jit(solution)/shard_map/dot_general | solution.py:486
  261.9 2.5 fusion.14
  264.4 3.4 copy.54
  267.8 0.5 fusion.23
  268.3 0.1 copy.43
  268.4 0.8 select_n.412.result_ref
  269.8 179.2 %collect.1 = bf16[256,16,128]{2,1,0:T(8,128)(2,1)S(1)} custom-call(s32[2,1904]{1,0:T(2,128)} %select_n.412.result_ref, s32[2,1904]{1,0:T(2,128)} %get-tuple-element.130.onward_ref, s32[3,256]{1,0:T(4,128)} %pad_add_fusion.final_ref, bf16[1024,16,128]{2,1,0:T(8,128)(2,1)} %bitcast.92), custom_call_target="tpu_custom_call" | custom-call | tf_op jit(solution)/shard_map/collect/pallas_call | solution.py:274
  449.0 0.3 conditional.1
  449.0 0.3 copy.60
  449.3 1.0 copy-done.1
  (62 shorter events, 2.3 us)
Async XLA Ops:
  0.0 46.3 %copy-start = (bf16[256,2048]{1,0:T(8,128)(2,1)S(1)}, bf16[256,2048]{1,0:T(8,128)(2,1)}, u32[]{:S(2)}) copy-start(bf16[256,2048]{1,0:T(8,128)(2,1)} %param.11) | copy-start | bytes 3145732
  10.3 54.3 %all-to-all-start.2 = ((f32[32,1,128]{2,1,0:T(1,128)}), f32[32,1,128]{2,1,0:T(1,128)S(1)}, u32[]{:S(2)}, u32[]{:S(2)}) async-start(f32[32,1,128]{2,1,0:T(1,128)} %bitcast.26), calls=%async_computation.2 | async-start | bytes 32768 | tf_op jit(solution)/shard_map/all_to_all | solution.py:532
  72.1 2.3 copy-start.2
  254.2 7.7 %copy-start.4 = (bf16[512,2048]{1,0:T(8,128)(2,1)S(1)}, bf16[512,2048]{1,0:T(8,128)(2,1)}, u32[]{:S(2)}) copy-start(bf16[512,2048]{1,0:T(8,128)(2,1)} %get-tuple-element.61) | copy-start | bytes 6291460
  264.4 5.4 %copy-start.3 = (f32[256,2]{0,1:T(2,128)S(1)}, f32[256,2]{0,1:T(2,128)}, u32[]{:S(2)}) copy-start(f32[256,2]{0,1:T(2,128)} %param.14) | copy-start | bytes 6148
  449.3 1.0 copy-start.1
